TPU v7x, 32 devices: a whole 2x2x4 slice. The times are simulated.
32 devices in a mesh: grp: 2 (over y), sp: 4 (over z), dp: 4 (over x, core).
Axes of the slice: x: 2, y: 2, z: 4, core: 2. Of those that a mesh axis runs over, the one named last changes fastest.
Arguments:
- tokens: bfloat16 [8, 640, 2048], P(('grp', 'dp'), 'sp'), parts along dimension 0, may hold values from -6 to 6
- query_weight: bfloat16 [2048, 1024], P('dp'), may hold values from -0.125 to 0.125
- key_weight: bfloat16 [2048, 256], P('dp'), may hold values from -0.125 to 0.125
- value_weight: bfloat16 [2048, 256], P('dp'), may hold values from -0.125 to 0.125
- out_weight: bfloat16 [1024, 2048], P(None, 'dp'), may hold values from -0.1875 to 0.1875
- query_gain: float32 [64], replicated, may hold values from 0.28 to 6
- key_gain: float32 [64], replicated, may hold values from 0.28 to 6
Outputs:
- mixed: bfloat16 [8, 640, 2048], P(('grp', 'dp'), 'sp'), parts along dimension 0
There are 2 independent parts, one for each index of `grp`. A program takes and returns all parts, laid end to end along the dimension named above; an argument that names none is the same for every part. Nothing has to cross between parts.
All inputs are finite; a program needn't handle non-finite values.
Results may differ from a plain program's by a relative error of at most 0.006.
The roundings to bfloat16 on the way count: a program that leaves them out, or rounds other values in their place, can miss the bound.
Values may be sent and summed in bfloat16 or wider, within the bound.
A program may use at most 64 MiB of HBM per device.

v0:
```python
import functools
import math

import jax
import jax.numpy as jnp
from jax import lax
from jax.experimental import pallas as pl
from jax.experimental.pallas import tpu as pltpu
from jax.sharding import PartitionSpec as P

HEADS = 16
KV_HEADS = 4
HEAD_DIM = 64
GRID_W = 64
LANES = 128

theta_base = 10000.0
norm_eps = 1e-06

BF = jnp.bfloat16
F32 = jnp.float32
MESH = pl.DeviceIdType.MESH


def rotary_tables(start, rows):
    quarter = HEAD_DIM // 4
    lane = lax.broadcasted_iota(jnp.int32, (rows, LANES), 1)
    position = start + lax.broadcasted_iota(jnp.int32, (rows, LANES), 0)
    step = lax.rem(lane, quarter).astype(F32)
    inverse = jnp.exp(step * (-math.log(theta_base) / quarter))
    grid_row = lax.div(position, GRID_W)
    grid_col = lax.rem(position, GRID_W)
    place = jnp.where(lax.rem(lane, 2 * quarter) < quarter, grid_row, grid_col).astype(F32)
    angles = place * inverse
    sine = jnp.sin(angles)
    return jnp.cos(angles), jnp.where(lax.rem(lane, HEAD_DIM) < HEAD_DIM // 2, -sine, sine)


def dot(a, b):
    return jnp.dot(a, b, preferred_element_type=F32)


def kernel(n, groups, seqs, cuts, order, tok, wk, wv, wq, wo, gq, gk, out,
           fk, fv, fq, fo, cos, sin, kv, acc_k, acc_v, acc_q, qs, k2, v2, att,
           xs, xr, ys, yr, ps, pr, os_, or_, cxs, cxr, zs, zr):
    d = lax.axis_index("dp")
    g = lax.axis_index("grp")
    s = lax.axis_index("sp")
    chips = n // 2
    mate = d + 1 - 2 * lax.rem(d, 2)
    own = (wk, wv, wq, wo)
    full = (fk, fv, fq, fo)
    rows = tok.shape[0]

    def hop(j):
        return lax.rem(d + 2 * j, n)

    def back(dev, j):
        return lax.rem(dev + n - 2 * j, n)

    def other(i):
        return i + 1 - 2 * lax.rem(i, 2)

    e = lax.rem(s, 2)
    colors = (2 * g + e, 2 * other(g) + e, 2 * g + other(e), 2 * other(g) + other(e))

    barrier = pltpu.get_barrier_semaphore()
    for j in range(1, chips):
        pl.semaphore_signal(barrier, inc=1, device_id={"dp": hop(j)}, device_id_type=MESH)
    for i in range(1, groups):
        pl.semaphore_signal(barrier, inc=1, device_id={"grp": lax.rem(g + i, groups)}, device_id_type=MESH)
    for i in range(1, seqs):
        pl.semaphore_signal(barrier, inc=1, device_id={"sp": lax.rem(s + i, seqs)}, device_id_type=MESH)
    pl.semaphore_signal(barrier, inc=1, device_id={"dp": mate}, device_id_type=MESH)
    pl.semaphore_wait(barrier, chips - 1 + groups - 1 + seqs - 1 + 1)

    sent = []

    def send(src, dst, ssem, rsem, where):
        copy = pltpu.make_async_remote_copy(
            src_ref=src, dst_ref=dst, send_sem=ssem, recv_sem=rsem, device_id=where, device_id_type=MESH)
        copy.start()
        sent.append(copy)

    def arrive(dst, ssem, rsem):
        pltpu.make_async_remote_copy(
            src_ref=dst, dst_ref=dst, send_sem=ssem, recv_sem=rsem,
            device_id={"dp": mate}, device_id_type=MESH).wait_recv()

    pieces = [(kind, cut) for kind in range(4) for cut in range(cuts[kind])]

    def block(ref, p, color):
        kind, cut = pieces[p]
        quarter = own[kind].shape[0] // 4
        size = quarter // cuts[kind]
        start = color * quarter + cut * size
        return ref.at[pl.ds(pl.multiple_of(start, 16), size)]

    def held(owner, p, rel):
        return block(full[pieces[p][0]].at[owner], p, colors[rel])

    ahead = 4

    def x_copy(index, j):
        p, rel = order[index]
        return pltpu.make_async_remote_copy(
            src_ref=block(own[pieces[p][0]], p, colors[rel]), dst_ref=held(d, p, rel),
            send_sem=xs.at[j - 1, rel, p], recv_sem=xr.at[j - 1, rel, p],
            device_id={"dp": hop(j)}, device_id_type=MESH)

    for index in range(min(ahead, len(order))):
        for j in range(1, chips):
            x_copy(index, j).start()
    for kind in range(4):
        send(own[kind], full[kind].at[d], os_.at[kind], or_.at[kind], {"dp": mate})

    def to_mate(here, j, rel, p):
        send(here, here, cxs.at[j - 1, rel, p], cxr.at[j - 1, rel, p], {"dp": mate})

    def step_x(p, rel):
        index = order.index((p, rel))
        for j in range(1, chips):
            here = held(back(d, j), p, rel)
            arrive(here, xs.at[j - 1, rel, p], xr.at[j - 1, rel, p])
            if rel != 3:
                send(here, here, ys.at[j - 1, rel // 2, p], yr.at[j - 1, rel // 2, p], {"grp": other(g)})
            if rel == 0 and (p, 2) not in order:
                send(here, here, ps.at[j - 1, p], pr.at[j - 1, p], {"sp": other(s)})
            to_mate(here, j, rel, p)
        for j in range(1, chips):
            x_copy(index, j).wait_send()
            if index + ahead < len(order):
                x_copy(index + ahead, j).start()

    def step_y(p, rel=1):
        for j in range(1, chips):
            here = held(back(d, j), p, rel)
            arrive(here, ys.at[j - 1, rel // 3, p], yr.at[j - 1, rel // 3, p])
            to_mate(here, j, rel, p)

    def step_z(p):
        for j in range(1, chips):
            here = held(back(d, j), p, 2)
            arrive(here, ps.at[j - 1, p], pr.at[j - 1, p])
            if (p, 3) not in order:
                send(here, here, ys.at[j - 1, 1, p], yr.at[j - 1, 1, p], {"grp": other(g)})
            to_mate(here, j, 2, p)

    def step_own(kind):
        arrive(full[kind].at[mate], os_.at[kind], or_.at[kind])

    def step_c(p):
        for j in range(1, chips):
            for rel in range(4):
                arrive(held(back(mate, j), p, rel), cxs.at[j - 1, rel, p], cxr.at[j - 1, rel, p])

    depth = wq.shape[0]

    def columns(owner):
        return pl.ds(pl.multiple_of(owner * depth, LANES), depth)

    def first(acc, ref):
        acc[...] = dot(tok[:, columns(d)], ref[...])

    def more(acc, ref, owner):
        acc[...] += dot(tok[:, columns(owner)], ref[owner])

    cos[...], sin[...] = rotary_tables(s * rows, rows)
    first(acc_k, wk)
    first(acc_v, wv)
    first(acc_q, wq)

    lane = lax.broadcasted_iota(jnp.int32, (rows, LANES), 1)
    low_half = lax.rem(lane, HEAD_DIM) < HEAD_DIM // 2
    low_head = lane < HEAD_DIM
    square_r = lax.broadcasted_iota(jnp.int32, (LANES, LANES), 0)
    square_c = lax.broadcasted_iota(jnp.int32, (LANES, LANES), 1)
    same_head = jnp.where(square_r // HEAD_DIM == square_c // HEAD_DIM, 1.0, 0.0).astype(BF)

    gain_k = jnp.concatenate([gk[...]] * 2, axis=1)
    gain_q = jnp.concatenate([gq[...]] * 2, axis=1)

    def norm_rotate(raw, gain):
        sq = raw * raw
        high = sq.astype(BF)
        low = (sq - high.astype(F32)).astype(BF)
        total = dot(high, same_head) + dot(low, same_head)
        scaled = raw * lax.rsqrt(total * (1.0 / HEAD_DIM) + norm_eps) * gain
        other = jnp.where(low_half, pltpu.roll(scaled, LANES - HEAD_DIM // 2, 1),
                          pltpu.roll(scaled, HEAD_DIM // 2, 1))
        return scaled * cos[...] + other * sin[...]

    others = [(d, j) for j in range(1, chips)] + [(mate, j) for j in range(1, chips)]

    held_back = []

    def relay(k):
        for way in range(2):
            sign = 2 * way - 1
            source, target = s + sign * k, s - sign
            here = (source >= 0) & (source < seqs)
            there = here & (target >= 0) & (target < seqs)
            slot = jnp.clip(source, 0, seqs - 1)
            goal = jnp.clip(target, 0, seqs - 1)
            width = kv.shape[2] // 2
            for half in range(2):
                ref = kv.at[slot, :, pl.ds(half * width, width)]
                if k > 0:
                    @pl.when(here)
                    def _():
                        arrive(ref, zs.at[way, half, k - 1], zr.at[way, half, k - 1])
                if k < seqs - 1:
                    copy = pltpu.make_async_remote_copy(
                        src_ref=ref, dst_ref=ref, send_sem=zs.at[way, half, k], recv_sem=zr.at[way, half, k],
                        device_id={"sp": goal}, device_id_type=MESH)
                    pl.when(there)(copy.start)
                    held_back.append((there, copy))

    def finish_kv():
        for acc, kind in ((acc_k, 0), (acc_v, 1)):
            for p in range(len(pieces)):
                if pieces[p][0] == kind:
                    step_c(p)
            for dev, j in others:
                more(acc, full[kind], back(dev, j))
        width = wk.shape[1]
        for t in range(width // LANES):
            cols = pl.ds(t * LANES, LANES)
            kv[s, :, cols] = norm_rotate(acc_k[:, cols], gain_k).astype(BF)
        kv[s, :, pl.ds(width, width)] = acc_v[...].astype(BF)
        relay(0)

    def finish_q():
        for p in range(len(pieces)):
            if pieces[p][0] == 2:
                step_c(p)
        for dev, j in others:
            more(acc_q, fq, back(dev, j))
        for t in range(wq.shape[1] // LANES):
            turned = norm_rotate(acc_q[:, pl.ds(t * LANES, LANES)], gain_q).astype(BF).astype(F32)
            turned = turned * HEAD_DIM ** (-0.5)
            qs[t, pl.ds(0, rows), :] = jnp.where(low_head, turned, 0.0).astype(BF)
            qs[t, pl.ds(rows, rows), :] = jnp.where(low_head, 0.0, turned).astype(BF)

    def gather_kv():
        width = wk.shape[1]
        for h in range(KV_HEADS):
            offset = (h % 2) * HEAD_DIM
            twice = jnp.where(square_r == offset + lax.rem(square_c, HEAD_DIM), 1.0, 0.0).astype(BF)
            base = (h // 2) * LANES
            for src, dst in ((base, k2), (width + base, v2)):
                both = kv[:, :, pl.ds(src, LANES)].reshape(seqs * rows, LANES)
                dst[h] = dot(both, twice).astype(BF)

    tiles = wq.shape[1] // LANES

    def attend(lo, hi):
        def body(t, carry):
            h = t // (tiles // KV_HEADS)
            scores = lax.dot_general(qs[t], k2[h], (((1,), (1,)), ((), ())), preferred_element_type=F32)
            top = jnp.max(scores, axis=-1, keepdims=True)
            weights = jnp.exp(scores - top)
            inverse = 1.0 / jnp.sum(weights, axis=-1, keepdims=True)
            mixed = dot((weights * inverse).astype(BF), v2[h])
            att[:, pl.ds(pl.multiple_of(t * LANES, LANES), LANES)] = jnp.where(
                low_head, mixed[:rows], mixed[rows:]).astype(BF)
            return carry
        lax.fori_loop(lo, hi, body, 0, unroll=True)

    def project(ref, owner):
        width = wo.shape[1]
        out[:, pl.ds(pl.multiple_of(owner * width, LANES), width)] = dot(att[...], ref).astype(BF)

    middle = max(1, (seqs - 1) // 3)
    step_x(0, 0)
    step_x(1, 0)
    step_x(0, 3)
    step_y(0, 1)
    step_z(0)
    step_x(1, 3)
    step_own(0)
    more(acc_k, fk, mate)
    step_own(1)
    more(acc_v, fv, mate)
    step_y(1, 1)
    step_z(1)
    step_x(2, 0)
    finish_kv()
    step_x(3, 0)
    step_own(2)
    more(acc_q, fq, mate)
    step_y(2, 1)
    step_z(2)
    for k in range(1, 1 + middle):
        relay(k)
    step_x(3, 3)
    step_y(3, 1)
    step_x(4, 0)
    step_z(3)
    step_y(2, 3)
    for k in range(1 + middle, 1 + 2 * middle):
        relay(k)
    step_x(5, 0)
    step_y(4, 1)
    finish_q()
    step_x(5, 2)
    step_z(4)
    for k in range(1 + 2 * middle, seqs):
        relay(k)
    step_x(4, 3)
    gather_kv()
    attend(tiles * 0 // 8, tiles * 2 // 8)
    step_y(5, 1)
    attend(tiles * 2 // 8, tiles * 4 // 8)
    step_y(5, 3)
    attend(tiles * 4 // 8, tiles * 8 // 8)
    project(wo[...], d)
    step_own(3)
    project(fo[mate], mate)
    for j in range(1, chips):
        project(fo[back(d, j)], back(d, j))
    for p in range(4, len(pieces)):
        step_c(p)
    for j in range(1, chips):
        project(fo[back(mate, j)], back(mate, j))
    for copy in sent:
        copy.wait_send()
    for there, copy in held_back:
        pl.when(there)(copy.wait_send)


def shards(n, groups, seqs, tokens, query_weight, key_weight, value_weight, out_weight, query_gain, key_gain):
    rows, width = tokens.shape[1], tokens.shape[2]
    local = tokens.reshape(rows, width)
    cuts = (1, 1, 2, 2)
    order = ((0, 0), (1, 0), (0, 3), (1, 3), (2, 0), (3, 0), (3, 3), (4, 0), (5, 0), (5, 2), (4, 3))
    count = sum(cuts)
    chips = n // 2
    kvw, qw = key_weight.shape[1], query_weight.shape[1]
    length = rows * seqs
    dma = pltpu.SemaphoreType.DMA
    vmem = pl.BlockSpec(memory_space=pltpu.VMEM)
    result = pl.pallas_call(
        functools.partial(kernel, n, groups, seqs, cuts, order),
        out_shape=jax.ShapeDtypeStruct((rows, width), BF),
        in_specs=[vmem] * 7,
        out_specs=vmem,
        scratch_shapes=[
            pltpu.VMEM((n,) + key_weight.shape, BF),
            pltpu.VMEM((n,) + value_weight.shape, BF),
            pltpu.VMEM((n,) + query_weight.shape, BF),
            pltpu.VMEM((n,) + out_weight.shape, BF),
            pltpu.VMEM((rows, LANES), F32),
            pltpu.VMEM((rows, LANES), F32),
            pltpu.VMEM((seqs, rows, 2 * kvw), BF),
            pltpu.VMEM((rows, kvw), F32),
            pltpu.VMEM((rows, kvw), F32),
            pltpu.VMEM((rows, qw), F32),
            pltpu.VMEM((qw // LANES, 2 * rows, LANES), BF),
            pltpu.VMEM((KV_HEADS, length, LANES), BF),
            pltpu.VMEM((KV_HEADS, length, LANES), BF),
            pltpu.VMEM((rows, qw), BF),
            dma((chips - 1, 4, count)), dma((chips - 1, 4, count)),
            dma((chips - 1, 2, count)), dma((chips - 1, 2, count)),
            dma((chips - 1, count)), dma((chips - 1, count)),
            dma((4,)), dma((4,)),
            dma((chips - 1, 4, count)), dma((chips - 1, 4, count)),
            dma((2, 2, seqs - 1)), dma((2, 2, seqs - 1)),
        ],
        compiler_params=pltpu.CompilerParams(
            collective_id=0, has_side_effects=True, vmem_limit_bytes=60 * 2 ** 20),
    )(local, key_weight, value_weight, query_weight, out_weight,
      query_gain.reshape(1, HEAD_DIM), key_gain.reshape(1, HEAD_DIM))
    return result.reshape(1, rows, width)


def solution(mesh):
    in_specs = (
        P(("grp", "dp"), "sp", None),
        P("dp", None),
        P("dp", None),
        P("dp", None),
        P(None, "dp"),
        P(),
        P(),
    )
    out_specs = P(("grp", "dp"), "sp", None)
    body = functools.partial(shards, mesh.shape["dp"], mesh.shape["grp"], mesh.shape["sp"])
    return jax.shard_map(body, mesh=mesh, in_specs=in_specs, out_specs=out_specs, check_vma=False)
```

profile of v0, /device:TPU:0, one launch (start us, length us, event | category | flops | bytes accessed | tf_op | source)
XLA Modules:
  0.0 48.2 jit_solution(17353948764420217796)
XLA Ops:
  0.0 46.2 %shard_map.73 = bf16[160,2048]{1,0:T(8,128)(2,1)} custom-call(bf16[160,2048]{1,0:T(8,128)(2,1)} %bitcast.5, bf16[512,256]{1,0:T(8,128)(2,1)} %wk.1, bf16[512,256]{1,0:T(8,128)(2,1)} %wv.1, bf16[512,1024]{1,0:T(8,128)(2,1)} %wq.1, bf16[1024,512]{1,0:T(8,128)(2,1)} %wo.1, f32[1,64]{1,0:T(1,128)} %bitcast.6, f32[1,64]{1,0:T(1,128)} %bitcast.7), custom_call_target="tpu_custom_call" | custom-call | tf_op jit(solution)/shard_map/pallas_call | solution.py:343
  46.2 2.0 %copy.9 = bf16[1,160,2048]{2,1,0:T(8,128)(2,1)} copy(bf16[1,160,2048]{2,1,0:T(8,128)(2,1)} %bitcast.4) | data formatting | bytes 1310720
where the time goes:
time: 48.4 us; the launch traced here: 48.2 us
  Pallas kernels  46.2 us (95%)
  local copies, waits for them, and re-layouts  1.98 us (4%)
    pallas_call x1, Pallas kernels, shards(): pl.pallas_call(functools.partial(kernel, n, groups, seqs, cuts, order), o...  46.2 us
    unnamed x1, local copies, waits for them, and re-layouts  1.98 us

commit v1 on v0

v1 whole, which is shorter than its diff:
```python
import functools
import math

import jax
import jax.numpy as jnp
from jax import lax
from jax.experimental import pallas as pl
from jax.experimental.pallas import tpu as pltpu
from jax.sharding import PartitionSpec as P

HEADS = 16
KV_HEADS = 4
HEAD_DIM = 64
GRID_W = 64
LANES = 128

theta_base = 10000.0
norm_eps = 1e-06

BF = jnp.bfloat16
F32 = jnp.float32
MESH = pl.DeviceIdType.MESH


def rotary_tables(start, rows):
    quarter = HEAD_DIM // 4
    lane = lax.broadcasted_iota(jnp.int32, (rows, LANES), 1)
    position = start + lax.broadcasted_iota(jnp.int32, (rows, LANES), 0)
    step = lax.rem(lane, quarter).astype(F32)
    inverse = jnp.exp(step * (-math.log(theta_base) / quarter))
    grid_row = lax.div(position, GRID_W)
    grid_col = lax.rem(position, GRID_W)
    place = jnp.where(lax.rem(lane, 2 * quarter) < quarter, grid_row, grid_col).astype(F32)
    angles = place * inverse
    sine = jnp.sin(angles)
    return jnp.cos(angles), jnp.where(lax.rem(lane, HEAD_DIM) < HEAD_DIM // 2, -sine, sine)


def dot(a, b):
    return jnp.dot(a, b, preferred_element_type=F32)


def kernel(n, groups, seqs, route, xlist, ylist, zlist, cq, co, tok_h, wk, wv, wq, wo, gq_h, gk_h, out,
           fk, fv, fq, fo, tok, gq, gk, cos, sin, kv, acc_k, acc_v, acc_q, qs, att,
           ls, os_, or_, xs, xr, ys, yr, zs, zr, cs, cr, hs, hr, fs):
    d = lax.axis_index("dp")
    g = lax.axis_index("grp")
    s = lax.axis_index("sp")
    chips = n // 2
    mate = d + 1 - 2 * lax.rem(d, 2)
    full = (fk, fv, fq, fo)
    rows = tok.shape[0]

    loads = []
    for i, (src, dst) in enumerate(((wk, fk.at[d]), (wv, fv.at[d]), (tok_h, tok), (wq, fq.at[d]), (wo, fo.at[d]),
                                    (gq_h, gq), (gk_h, gk))):
        copy = pltpu.make_async_copy(src, dst, ls.at[i])
        copy.start()
        loads.append(copy)

    def hop(j):
        return lax.rem(d + 2 * j, n)

    def back(dev, j):
        return lax.rem(dev + n - 2 * j, n)

    def other(i):
        return i + 1 - 2 * lax.rem(i, 2)

    def inside(i):
        return (i >= 0) & (i < seqs)

    def near(i):
        return jnp.clip(i, 0, seqs - 1)

    e = lax.rem(s, 2)
    colors = (2 * g + e, 2 * other(g) + e, 2 * g + other(e), 2 * other(g) + other(e))
    offsets = (2, -2, 1, -1)

    barrier = pltpu.get_barrier_semaphore()
    for j in range(1, chips):
        pl.semaphore_signal(barrier, inc=1, device_id={"dp": hop(j)}, device_id_type=MESH)
    for i in range(1, groups):
        pl.semaphore_signal(barrier, inc=1, device_id={"grp": lax.rem(g + i, groups)}, device_id_type=MESH)
    count = jnp.int32(chips - 1 + groups - 1 + 1)
    for o in offsets:
        def greet(o=o):
            pl.semaphore_signal(barrier, inc=1, device_id={"sp": near(s + o)}, device_id_type=MESH)
        pl.when(inside(s + o))(greet)
        count = count + inside(s + o).astype(jnp.int32)
    pl.semaphore_signal(barrier, inc=1, device_id={"dp": mate}, device_id_type=MESH)

    cos[...], sin[...] = rotary_tables(s * rows, rows)

    waits = []

    def remote(src, dst, ssem, rsem, where):
        return pltpu.make_async_remote_copy(
            src_ref=src, dst_ref=dst, send_sem=ssem, recv_sem=rsem, device_id=where, device_id_type=MESH)

    def arrive(dst, ssem, rsem):
        remote(dst, dst, ssem, rsem, {"dp": mate}).wait_recv()

    pieces = [(0, 0), (1, 0)] + [(2, c) for c in range(cq)] + [(3, c) for c in range(co)]
    cuts = (1, 1, cq, co)

    def part(owner, p, start, blocks):
        kind, cut = pieces[p]
        quarter = full[kind].shape[1] // 4
        width = full[kind].shape[2] // cuts[kind]
        ref = full[kind].at[owner]
        if isinstance(start, int):
            return ref.at[pl.ds(start * quarter, blocks * quarter), pl.ds(cut * width, width)]
        return ref.at[pl.ds(pl.multiple_of(start * quarter, 16), blocks * quarter), pl.ds(cut * width, width)]

    def held(owner, p, rel):
        return part(owner, p, colors[rel], 1)

    for copy in loads:
        copy.wait()
    pl.semaphore_wait(barrier, count)

    def x_send(index):
        p, rel = xlist[index]
        for j in range(1, chips):
            here = held(d, p, rel)
            remote(here, here, xs.at[j - 1, p], xr.at[j - 1, index], {"dp": hop(j)}).start()

    def own_send(kind):
        here = full[kind].at[d]
        remote(here, here, os_.at[kind], or_.at[kind], {"dp": mate}).start()

    ahead = 3
    for index in range(ahead):
        x_send(index)
    for kind in range(4):
        own_send(kind)
    for index in range(ahead, len(xlist)):
        x_send(index)

    def step(p, rel):
        way = route[p, rel]
        table, ssem, rsem = {"x": (xlist, xs, xr), "y": (ylist, ys, yr), "z": (zlist, zs, zr)}[way]
        for j in range(1, chips):
            here = held(back(d, j), p, rel)
            arrive(here, ssem.at[j - 1, 0], rsem.at[j - 1, table.index((p, rel))])
            if rel in (0, 1) and route[p, rel + 2] == "z":
                i = zlist.index((p, rel + 2))
                remote(here, here, zs.at[j - 1, zsend.index(p)], zr.at[j - 1, i], {"sp": other(s)}).start()
            if rel in (0, 2) and route[p, rel + 1] == "y":
                i = ylist.index((p, rel + 1))
                remote(here, here, ys.at[j - 1, p], yr.at[j - 1, i], {"grp": other(g)}).start()
            remote(here, here, cs.at[j - 1, p], cr.at[j - 1, p], {"dp": mate}).start()

    zsend = sorted({p for p, _ in zlist})

    def step_c(p):
        for j in range(1, chips):
            arrive(part(back(mate, j), p, 0, 4), cs.at[j - 1, p], cr.at[j - 1, p])

    def step_own(kind):
        arrive(full[kind].at[mate], os_.at[kind], or_.at[kind])

    def drain():
        for kind in range(4):
            here = full[kind].at[d]
            remote(here, here, os_.at[kind], or_.at[kind], {"dp": mate}).wait_send()
        for j in range(1, chips):
            for p in range(len(pieces)):
                for table, sem in ((xlist, xs.at[j - 1, p]), (ylist, ys.at[j - 1, p]),
                                   (zlist, zs.at[j - 1, zsend.index(p)] if p in zsend else None)):
                    blocks = len([1 for q, _ in table if q == p])
                    if blocks:
                        here = part(d, p, 0, blocks)
                        remote(here, here, sem, xr.at[0, 0], {"dp": mate}).wait_send()
                here = part(back(d, j), p, 0, 4)
                remote(here, here, cs.at[j - 1, p], cr.at[j - 1, p], {"dp": mate}).wait_send()
        for i, o in enumerate(offsets):
            here = kv.at[s]
            pl.when(inside(s + o))(remote(here, here, hs.at[i], hr.at[0, 0], {"dp": mate}).wait_send)
        for i, (way, k, o) in enumerate(relays):
            here = kv.at[near(s - way * k)]
            pl.when(inside(s - way * k) & inside(s + way * o))(
                remote(here, here, fs.at[i], hr.at[0, 0], {"dp": mate}).wait_send)

    relays = [(way, k, o) for way in (1, -1) for k in range(2, seqs, 2) for o in (1, 2) if k + o < seqs]
    half = kv.shape[2] // 2

    def slot(i, which):
        return kv.at[i, :, pl.ds(which * half, half)]

    def spread(which):
        for i, o in enumerate(offsets):
            here = slot(s, which)
            pl.when(inside(s + o))(
                remote(here, here, hs.at[i], hr.at[s, which], {"sp": near(s + o)}).start)

    def collect(which, k):
        for way in (1, -1):
            source = near(s - way * k)
            here = slot(source, which)

            def take(here=here, source=source):
                arrive(here, hs.at[0], hr.at[source, which])
            pl.when(inside(s - way * k))(take)
            for i, (w, kk, o) in enumerate(relays):
                if w == way and kk == k:
                    pl.when(inside(s - way * k) & inside(s + way * o))(
                        remote(here, here, fs.at[i], hr.at[source, which], {"sp": near(s + way * o)}).start)

    depth = fq.shape[1]

    def columns(owner):
        return pl.ds(pl.multiple_of(owner * depth, LANES), depth)

    def first(acc, ref):
        acc[...] = dot(tok[:, columns(d)], ref[d])

    def more(acc, ref, owner):
        acc[...] += dot(tok[:, columns(owner)], ref[owner])

    first(acc_k, fk)
    first(acc_v, fv)
    first(acc_q, fq)

    lane = lax.broadcasted_iota(jnp.int32, (rows, LANES), 1)
    low_half = lax.rem(lane, HEAD_DIM) < HEAD_DIM // 2
    low_head = lane < HEAD_DIM
    square_r = lax.broadcasted_iota(jnp.int32, (LANES, LANES), 0)
    square_c = lax.broadcasted_iota(jnp.int32, (LANES, LANES), 1)
    same_head = jnp.where(square_r // HEAD_DIM == square_c // HEAD_DIM, 1.0, 0.0).astype(BF)

    gain_k = jnp.concatenate([gk[...]] * 2, axis=1)
    gain_q = jnp.concatenate([gq[...]] * 2, axis=1)

    def norm_rotate(raw, gain):
        sq = raw * raw
        high = sq.astype(BF)
        low = (sq - high.astype(F32)).astype(BF)
        total = dot(high, same_head) + dot(low, same_head)
        scaled = raw * lax.rsqrt(total * (1.0 / HEAD_DIM) + norm_eps) * gain
        other = jnp.where(low_half, pltpu.roll(scaled, LANES - HEAD_DIM // 2, 1),
                          pltpu.roll(scaled, HEAD_DIM // 2, 1))
        return scaled * cos[...] + other * sin[...]

    others = [(d, j) for j in range(1, chips)] + [(mate, j) for j in range(1, chips)]

    def finish_k():
        step_c(0)
        for dev, j in others:
            more(acc_k, fk, back(dev, j))
        for t in range(half // LANES):
            cols = pl.ds(t * LANES, LANES)
            kv[s, :, cols] = norm_rotate(acc_k[:, cols], gain_k).astype(BF)

    def finish_v():
        step_c(1)
        for dev, j in others:
            more(acc_v, fv, back(dev, j))
        kv[s, :, pl.ds(half, half)] = acc_v[...].astype(BF)

    tiles = fq.shape[2] // LANES
    group = HEADS // KV_HEADS

    def finish_q(cut):
        step_c(2 + cut)
        width = fq.shape[2] // cq
        cols = pl.ds(cut * width, width)
        for dev, j in others:
            owner = back(dev, j)
            acc_q[:, cols] += dot(tok[:, columns(owner)], fq[owner, :, cols])
        for t in range(cut * tiles // cq, (cut + 1) * tiles // cq):
            turned = norm_rotate(acc_q[:, pl.ds(t * LANES, LANES)], gain_q).astype(BF).astype(F32)
            turned = turned * HEAD_DIM ** (-0.5)
            swapped = pltpu.roll(turned, HEAD_DIM, 1)
            if (2 * t // group) % 2 == 0:
                one, two = jnp.where(low_head, turned, 0.0), jnp.where(low_head, swapped, 0.0)
            else:
                one, two = jnp.where(low_head, 0.0, swapped), jnp.where(low_head, 0.0, turned)
            qs[t, pl.ds(0, rows), :] = one.astype(BF)
            qs[t, pl.ds(rows, rows), :] = two.astype(BF)

    def attend(lo, hi):
        for t in range(lo, hi):
            h = 2 * t // group
            base = (h // 2) * LANES
            keys = kv[:, :, pl.ds(base, LANES)].reshape(seqs * rows, LANES)
            values = kv[:, :, pl.ds(half + base, LANES)].reshape(seqs * rows, LANES)
            scores = lax.dot_general(qs[t], keys, (((1,), (1,)), ((), ())), preferred_element_type=F32)
            top = jnp.max(scores, axis=-1, keepdims=True)
            weights = jnp.exp(scores - top)
            inverse = 1.0 / jnp.sum(weights, axis=-1, keepdims=True)
            mixed = dot((weights * inverse).astype(BF), values)
            one, two = mixed[:rows], mixed[rows:]
            if h % 2 == 0:
                two = pltpu.roll(two, HEAD_DIM, 1)
            else:
                one = pltpu.roll(one, HEAD_DIM, 1)
            att[:, pl.ds(t * LANES, LANES)] = jnp.where(low_head, one, two).astype(BF)

    def project(owner, lo, hi):
        width = fo.shape[2]
        size = (hi - lo) * (width // co)
        offset = lo * (width // co)
        out[:, pl.ds(pl.multiple_of(owner * width + offset, LANES), size)] = dot(
            att[...], fo[owner, :, pl.ds(offset, size)]).astype(BF)

    Q = [2 + c for c in range(cq)]
    O = [2 + cq + c for c in range(co)]
    q0, q1 = Q[0], Q[-1]

    def od(i, rel):
        if i < co:
            step(O[i], rel)

    step(0, 0)
    step(1, 0)
    step_own(0)
    more(acc_k, fk, mate)
    step_own(1)
    more(acc_v, fv, mate)
    step(0, 3)
    step(0, 1)
    step(0, 2)
    finish_k()
    spread(0)
    step(1, 1)
    step(1, 2)
    step(q0, 0)
    step_own(2)
    more(acc_q, fq, mate)
    step(1, 3)
    finish_v()
    spread(1)
    collect(0, 2)
    step(q0, 2)
    step(q0, 1)
    step(q1, 0)
    collect(1, 2)
    step(q0, 3)
    step(q1, 2)
    finish_q(0)
    od(0, 0)
    step(q1, 1)
    od(1, 0)
    [collect(0, k) for k in range(1, seqs) if k != 2]
    [collect(1, k) for k in range(1, seqs) if k != 2]
    od(2, 0)
    attend(0, tiles // 4)
    step(q1, 3)
    od(3, 0)
    od(0, 2)
    attend(tiles // 4, tiles // 2)
    od(0, 1)
    od(1, 2)
    finish_q(1)
    attend(tiles // 2, tiles * 3 // 4)
    od(1, 1)
    od(2, 2)
    od(1, 3)
    attend(tiles * 3 // 4, tiles)
    od(2, 1)
    od(3, 2)
    od(2, 3)
    project(d, 0, co)
    step_own(3)
    project(mate, 0, co)
    od(3, 1)
    od(3, 3)
    od(0, 3)
    [project(back(d, j), 0, co) for j in range(1, chips)]
    for p in O:
        step_c(p)
    for j in range(1, chips):
        project(back(mate, j), 0, co)
    drain()


def shards(n, groups, seqs, tokens, query_weight, key_weight, value_weight, out_weight, query_gain, key_gain):
    rows, width = tokens.shape[1], tokens.shape[2]
    local = tokens.reshape(rows, width)
    chips = n // 2
    kvw, qw = key_weight.shape[1], query_weight.shape[1]
    cq = 2
    co = max(1, min(4, out_weight.shape[1] // LANES))
    pieces = 2 + cq + co
    Q = range(2, 2 + cq)
    O = range(2 + cq, pieces)
    xlist = [(0, 0), (1, 0), (0, 3)] + [(p, r) for p in Q for r in (0, 2)] + [(p, 0) for p in O] + [
        (p, 3) for p in O[1:]]
    ylist = [(0, 1), (1, 1), (1, 3)] + [(p, r) for p in Q for r in (1, 3)] + [(p, 1) for p in O]
    zlist = [(0, 2), (1, 2)] + [(p, 2) for p in O] + [(O[0], 3)]
    route = {**{k: "x" for k in xlist}, **{k: "y" for k in ylist}, **{k: "z" for k in zlist}}
    zsends = len({p for p, _ in zlist})
    relays = 2 * len([1 for k in range(2, seqs, 2) for o in (1, 2) if k + o < seqs])
    dma = pltpu.SemaphoreType.DMA
    vmem = pl.BlockSpec(memory_space=pltpu.VMEM)
    hbm = pl.BlockSpec(memory_space=pltpu.HBM)
    result = pl.pallas_call(
        functools.partial(kernel, n, groups, seqs, route, xlist, ylist, zlist, cq, co),
        out_shape=pltpu.VMEM((rows, width), BF),
        in_specs=[hbm] * 7,
        out_specs=vmem,
        scratch_shapes=[
            pltpu.VMEM((n,) + key_weight.shape, BF),
            pltpu.VMEM((n,) + value_weight.shape, BF),
            pltpu.VMEM((n,) + query_weight.shape, BF),
            pltpu.VMEM((n,) + out_weight.shape, BF),
            pltpu.VMEM((rows, width), BF),
            pltpu.VMEM((1, HEAD_DIM), F32),
            pltpu.VMEM((1, HEAD_DIM), F32),
            pltpu.VMEM((rows, LANES), F32),
            pltpu.VMEM((rows, LANES), F32),
            pltpu.VMEM((seqs, rows, 2 * kvw), BF),
            pltpu.VMEM((rows, kvw), F32),
            pltpu.VMEM((rows, kvw), F32),
            pltpu.VMEM((rows, qw), F32),
            pltpu.VMEM((qw // LANES, 2 * rows, LANES), BF),
            pltpu.VMEM((rows, qw), BF),
            dma((7,)), dma((4,)), dma((4,)),
            dma((chips - 1, pieces)), dma((chips - 1, len(xlist))),
            dma((chips - 1, pieces)), dma((chips - 1, len(ylist))),
            dma((chips - 1, zsends)), dma((chips - 1, len(zlist))),
            dma((chips - 1, pieces)), dma((chips - 1, pieces)),
            dma((4,)), dma((seqs, 2)), dma((max(1, relays),)),
        ],
        compiler_params=pltpu.CompilerParams(
            collective_id=0, has_side_effects=True, vmem_limit_bytes=40 * 2 ** 20),
    )(*[pltpu.with_memory_space_constraint(a, pltpu.HBM) for a in (
        local, key_weight, value_weight, query_weight, out_weight,
        query_gain.reshape(1, HEAD_DIM), key_gain.reshape(1, HEAD_DIM))])
    return result.reshape(1, rows, width)


def solution(mesh):
    in_specs = (
        P(("grp", "dp"), "sp", None),
        P("dp", None),
        P("dp", None),
        P("dp", None),
        P(None, "dp"),
        P(),
        P(),
    )
    out_specs = P(("grp", "dp"), "sp", None)
    body = functools.partial(shards, mesh.shape["dp"], mesh.shape["grp"], mesh.shape["sp"])
    return jax.shard_map(body, mesh=mesh, in_specs=in_specs, out_specs=out_specs, check_vma=False)
```

time: 48.4 us -> 39.8 us (0.82)
  Pallas kernels: 46.2 us -> 38.7 us
  local copies, waits for them, and re-layouts: 1.98 us -> 0.84 us
    pallas_call x1, Pallas kernels: 46.2 us -> 38.7 us  [shards(): pl.pallas_call(functools.partial(kernel, n, groups, seqs, route, xlist, y...]
    unnamed x1, local copies, waits for them, and re-layouts: 1.98 us -> 0.84 us
where the time goes in v1:
time: 39.8 us; the launch traced here: 39.5 us
  Pallas kernels  38.7 us (97%)
  local copies, waits for them, and re-layouts  0.84 us (2%)
    pallas_call x1, Pallas kernels, shards(): pl.pallas_call(functools.partial(kernel, n, groups, seqs, route, xlist, y...  38.7 us
    unnamed x1, local copies, waits for them, and re-layouts  0.84 us

profile of v1, /device:TPU:0, one launch (start us, length us, event | category | flops | bytes accessed | tf_op | source)
XLA Modules:
  0.0 39.5 jit_solution(4738816447710091337)
XLA Ops:
  0.0 38.7 %shard_map.73 = bf16[160,2048]{1,0:T(8,128)(2,1)S(1)} custom-call(bf16[160,2048]{1,0:T(8,128)(2,1)} %bitcast.5, bf16[512,256]{1,0:T(8,128)(2,1)} %wk.1, bf16[512,256]{1,0:T(8,128)(2,1)} %wv.1, bf16[512,1024]{1,0:T(8,128)(2,1)} %wq.1, bf16[1024,512]{1,0:T(8,128)(2,1)} %wo.1, f32[1,64]{1,0:T(1,128)} %bitcast.6, f32[1,64]{1,0:T(1,128)} %bitcast.7), custom_call_target="tpu_custom_call" | custom-call | tf_op jit(solution)/shard_map/pallas_call | solution.py:399
  38.7 0.8 %copy.9 = bf16[1,160,2048]{2,1,0:T(8,128)(2,1)} copy(bf16[1,160,2048]{2,1,0:T(8,128)(2,1)S(1)} %bitcast.4) | data formatting | bytes 1310720

commit v2 on v1

--- a/solution.py
+++ b/solution.py
@@ -39,10 +39,14 @@
 def dot(a, b):
     return jnp.dot(a, b, preferred_element_type=F32)
 
+X_PIECES = ((0, 0, 0), (1, 0, 0), (2, 0, 0), (0, 0, 3), (2, 1, 0), (2, 3, 0), (2, 1, 2), (2, 2, 2), (3, 2, 0), (3, 1, 0), (3, 0, 2), (2, 2, 0), (3, 3, 1), (2, 2, 1), (3, 3, 2), (3, 1, 2), (3, 0, 0), (3, 3, 0), (3, 0, 1))
+Y_PIECES = ((0, 0, 1), (1, 0, 1), (1, 0, 3), (2, 0, 1), (2, 0, 3), (2, 1, 1), (2, 1, 3), (2, 2, 3), (2, 3, 1), (2, 3, 3), (3, 0, 3), (3, 1, 1), (3, 2, 1), (3, 2, 3))
+Z_PIECES = ((0, 0, 2), (1, 0, 2), (2, 0, 2), (2, 3, 2), (3, 1, 3), (3, 2, 2), (3, 3, 3))
+
 
 def kernel(n, groups, seqs, route, xlist, ylist, zlist, cq, co, tok_h, wk, wv, wq, wo, gq_h, gk_h, out,
-           fk, fv, fq, fo, tok, gq, gk, cos, sin, kv, acc_k, acc_v, acc_q, qs, att,
-           ls, os_, or_, xs, xr, ys, yr, zs, zr, cs, cr, hs, hr, fs):
+           fk, fv, fq, fo, tok, gq, gk, cos, sin, kv, acc_k, acc_v, acc_q, qs, att, probs,
+           ls, os_, or_, xs, xr, ys, yr, zs, zr, cs, cr, hs, hr, fs, ready):
     d = lax.axis_index("dp")
     g = lax.axis_index("grp")
     s = lax.axis_index("sp")
@@ -83,7 +87,7 @@
     for i in range(1, groups):
         pl.semaphore_signal(barrier, inc=1, device_id={"grp": lax.rem(g + i, groups)}, device_id_type=MESH)
     count = jnp.int32(chips - 1 + groups - 1 + 1)
-    for o in offsets:
+    for o in (1, -1):
         def greet(o=o):
             pl.semaphore_signal(barrier, inc=1, device_id={"sp": near(s + o)}, device_id_type=MESH)
         pl.when(inside(s + o))(greet)
@@ -103,6 +107,8 @@
 
     pieces = [(0, 0), (1, 0)] + [(2, c) for c in range(cq)] + [(3, c) for c in range(co)]
     cuts = (1, 1, cq, co)
+
+    shelf = [kind if kind < 2 else 2 + 2 * c // cq if kind == 2 else 4 for kind, c in pieces]
 
     def part(owner, p, start, blocks):
         kind, cut = pieces[p]
@@ -120,22 +126,26 @@
         copy.wait()
     pl.semaphore_wait(barrier, count)
 
+    for i, o in enumerate((1, -1)):
+        def vouch(i=i, o=o):
+            pl.semaphore_signal(ready.at[i], inc=1, device_id={"sp": near(s + o)}, device_id_type=MESH)
+        pl.when(inside(s + o) & inside(s - o))(vouch)
+
     def x_send(index):
         p, rel = xlist[index]
         for j in range(1, chips):
             here = held(d, p, rel)
-            remote(here, here, xs.at[j - 1, p], xr.at[j - 1, index], {"dp": hop(j)}).start()
+            remote(here, here, xs.at[j - 1, pieces[p][0]], xr.at[j - 1, index], {"dp": hop(j)}).start()
 
     def own_send(kind):
         here = full[kind].at[d]
         remote(here, here, os_.at[kind], or_.at[kind], {"dp": mate}).start()
 
-    ahead = 3
-    for index in range(ahead):
+    for index in range(4):
         x_send(index)
     for kind in range(4):
         own_send(kind)
-    for index in range(ahead, len(xlist)):
+    for index in range(4, len(xlist)):
         x_send(index)
 
     def step(p, rel):
@@ -146,17 +156,17 @@
             arrive(here, ssem.at[j - 1, 0], rsem.at[j - 1, table.index((p, rel))])
             if rel in (0, 1) and route[p, rel + 2] == "z":
                 i = zlist.index((p, rel + 2))
-                remote(here, here, zs.at[j - 1, zsend.index(p)], zr.at[j - 1, i], {"sp": other(s)}).start()
+                remote(here, here, zs.at[j - 1, pieces[p][0]], zr.at[j - 1, i], {"sp": other(s)}).start()
             if rel in (0, 2) and route[p, rel + 1] == "y":
                 i = ylist.index((p, rel + 1))
-                remote(here, here, ys.at[j - 1, p], yr.at[j - 1, i], {"grp": other(g)}).start()
-            remote(here, here, cs.at[j - 1, p], cr.at[j - 1, p], {"dp": mate}).start()
-
-    zsend = sorted({p for p, _ in zlist})
-
-    def step_c(p):
+                remote(here, here, ys.at[j - 1, pieces[p][0]], yr.at[j - 1, i], {"grp": other(g)}).start()
+            remote(here, here, cs.at[j - 1, pieces[p][0]], cr.at[j - 1, shelf[p]], {"dp": mate}).start()
+
+    def step_c(kind, lo, hi):
+        width = full[kind].shape[2] // cuts[kind]
         for j in range(1, chips):
-            arrive(part(back(mate, j), p, 0, 4), cs.at[j - 1, p], cr.at[j - 1, p])
+            arrive(full[kind].at[back(mate, j), :, pl.ds(lo * width, (hi - lo) * width)],
+                   cs.at[j - 1, kind], cr.at[j - 1, shelf[pieces.index((kind, lo))]])
 
     def step_own(kind):
         arrive(full[kind].at[mate], os_.at[kind], or_.at[kind])
@@ -166,15 +176,14 @@
             here = full[kind].at[d]
             remote(here, here, os_.at[kind], or_.at[kind], {"dp": mate}).wait_send()
         for j in range(1, chips):
-            for p in range(len(pieces)):
-                for table, sem in ((xlist, xs.at[j - 1, p]), (ylist, ys.at[j - 1, p]),
-                                   (zlist, zs.at[j - 1, zsend.index(p)] if p in zsend else None)):
-                    blocks = len([1 for q, _ in table if q == p])
+            for kind in range(4):
+                for table, sem in ((xlist, xs), (ylist, ys), (zlist, zs)):
+                    blocks = len([1 for q, _ in table if pieces[q][0] == kind])
                     if blocks:
-                        here = part(d, p, 0, blocks)
-                        remote(here, here, sem, xr.at[0, 0], {"dp": mate}).wait_send()
-                here = part(back(d, j), p, 0, 4)
-                remote(here, here, cs.at[j - 1, p], cr.at[j - 1, p], {"dp": mate}).wait_send()
+                        here = full[kind].at[d, pl.ds(0, blocks * (full[kind].shape[1] // 4) // cuts[kind])]
+                        remote(here, here, sem.at[j - 1, kind], xr.at[0, 0], {"dp": mate}).wait_send()
+                here = full[kind].at[d]
+                remote(here, here, cs.at[j - 1, kind], cr.at[j - 1, 0], {"dp": mate}).wait_send()
         for i, o in enumerate(offsets):
             here = kv.at[s]
             pl.when(inside(s + o))(remote(here, here, hs.at[i], hr.at[0, 0], {"dp": mate}).wait_send)
@@ -189,24 +198,44 @@
     def slot(i, which):
         return kv.at[i, :, pl.ds(which * half, half)]
 
+    def met():
+        for i, o in enumerate((1, -1)):
+            def heard(i=i):
+                pl.semaphore_wait(ready.at[i], 1)
+            pl.when(inside(s - o) & inside(s - 2 * o))(heard)
+
     def spread(which):
         for i, o in enumerate(offsets):
             here = slot(s, which)
             pl.when(inside(s + o))(
                 remote(here, here, hs.at[i], hr.at[s, which], {"sp": near(s + o)}).start)
 
-    def collect(which, k):
+    def onward(way, k):
+        return functools.reduce(lambda a, b: a | b, [inside(s + way * o) for w, kk, o in relays if (w, kk) == (way, k)])
+
+    def take(which, way, k):
+        source = near(s - way * k)
+        arrive(slot(source, which), hs.at[0], hr.at[source, which])
+
+    def relay(which, k):
         for way in (1, -1):
+            if not [1 for w, kk, o in relays if (w, kk) == (way, k)]:
+                continue
             source = near(s - way * k)
             here = slot(source, which)
-
-            def take(here=here, source=source):
-                arrive(here, hs.at[0], hr.at[source, which])
-            pl.when(inside(s - way * k))(take)
+            pl.when(inside(s - way * k) & onward(way, k))(functools.partial(take, which, way, k))
             for i, (w, kk, o) in enumerate(relays):
-                if w == way and kk == k:
+                if (w, kk) == (way, k):
                     pl.when(inside(s - way * k) & inside(s + way * o))(
                         remote(here, here, fs.at[i], hr.at[source, which], {"sp": near(s + way * o)}).start)
+
+    def collect(which):
+        for k in range(1, seqs):
+            for way in (1, -1):
+                need = inside(s - way * k)
+                if [1 for w, kk, o in relays if (w, kk) == (way, k)]:
+                    need = need & jnp.logical_not(onward(way, k))
+                pl.when(need)(functools.partial(take, which, way, k))
 
     depth = fq.shape[1]
 
@@ -246,7 +275,7 @@
     others = [(d, j) for j in range(1, chips)] + [(mate, j) for j in range(1, chips)]
 
     def finish_k():
-        step_c(0)
+        step_c(0, 0, 1)
         for dev, j in others:
             more(acc_k, fk, back(dev, j))
         for t in range(half // LANES):
@@ -254,7 +283,7 @@
             kv[s, :, cols] = norm_rotate(acc_k[:, cols], gain_k).astype(BF)
 
     def finish_v():
-        step_c(1)
+        step_c(1, 0, 1)
         for dev, j in others:
             more(acc_v, fv, back(dev, j))
         kv[s, :, pl.ds(half, half)] = acc_v[...].astype(BF)
@@ -262,16 +291,15 @@
     tiles = fq.shape[2] // LANES
     group = HEADS // KV_HEADS
 
-    def finish_q(cut):
-        step_c(2 + cut)
-        width = fq.shape[2] // cq
-        cols = pl.ds(cut * width, width)
+    def finish_q(part_):
+        step_c(2, part_ * cq // 2, (part_ + 1) * cq // 2)
+        width = fq.shape[2] // 2
+        cols = pl.ds(part_ * width, width)
         for dev, j in others:
             owner = back(dev, j)
             acc_q[:, cols] += dot(tok[:, columns(owner)], fq[owner, :, cols])
-        for t in range(cut * tiles // cq, (cut + 1) * tiles // cq):
-            turned = norm_rotate(acc_q[:, pl.ds(t * LANES, LANES)], gain_q).astype(BF).astype(F32)
-            turned = turned * HEAD_DIM ** (-0.5)
+        for t in range(part_ * tiles // 2, (part_ + 1) * tiles // 2):
+            turned = norm_rotate(acc_q[:, pl.ds(t * LANES, LANES)], gain_q * HEAD_DIM ** (-0.5))
             swapped = pltpu.roll(turned, HEAD_DIM, 1)
             if (2 * t // group) % 2 == 0:
                 one, two = jnp.where(low_head, turned, 0.0), jnp.where(low_head, swapped, 0.0)
@@ -280,23 +308,38 @@
             qs[t, pl.ds(0, rows), :] = one.astype(BF)
             qs[t, pl.ds(rows, rows), :] = two.astype(BF)
 
-    def attend(lo, hi):
-        for t in range(lo, hi):
-            h = 2 * t // group
-            base = (h // 2) * LANES
-            keys = kv[:, :, pl.ds(base, LANES)].reshape(seqs * rows, LANES)
-            values = kv[:, :, pl.ds(half + base, LANES)].reshape(seqs * rows, LANES)
-            scores = lax.dot_general(qs[t], keys, (((1,), (1,)), ((), ())), preferred_element_type=F32)
-            top = jnp.max(scores, axis=-1, keepdims=True)
-            weights = jnp.exp(scores - top)
-            inverse = 1.0 / jnp.sum(weights, axis=-1, keepdims=True)
-            mixed = dot((weights * inverse).astype(BF), values)
-            one, two = mixed[:rows], mixed[rows:]
+    def softmax(h):
+        base = (h // 2) * LANES
+        keys = kv[:, :, pl.ds(base, LANES)].reshape(seqs * rows, LANES)
+        lo, count = h * tiles // KV_HEADS, tiles // KV_HEADS
+        asked = qs[lo:lo + count].reshape(count * 2 * rows, LANES)
+        scores = lax.dot_general(asked, keys, (((1,), (1,)), ((), ())), preferred_element_type=F32)
+        top = jnp.max(scores, axis=-1, keepdims=True)
+        weights = jnp.exp(scores - top)
+        inverse = 1.0 / jnp.sum(weights, axis=-1, keepdims=True)
+        return (weights * inverse).astype(BF)
+
+    def mix(h, weights):
+        base = (h // 2) * LANES
+        lo, count = h * tiles // KV_HEADS, tiles // KV_HEADS
+        values = kv[:, :, pl.ds(half + base, LANES)].reshape(seqs * rows, LANES)
+        mixed = dot(weights, values)
+        for i in range(count):
+            one, two = mixed[2 * i * rows:(2 * i + 1) * rows], mixed[(2 * i + 1) * rows:(2 * i + 2) * rows]
             if h % 2 == 0:
                 two = pltpu.roll(two, HEAD_DIM, 1)
             else:
                 one = pltpu.roll(one, HEAD_DIM, 1)
-            att[:, pl.ds(t * LANES, LANES)] = jnp.where(low_head, one, two).astype(BF)
+            att[:, pl.ds((lo + i) * LANES, LANES)] = jnp.where(low_head, one, two).astype(BF)
+
+    def soft(h):
+        probs[h] = softmax(h)
+
+    def blend(h):
+        mix(h, probs[h])
+
+    def heads(h):
+        mix(h, softmax(h))
 
     def project(owner, lo, hi):
         width = fo.shape[2]
@@ -307,70 +350,82 @@
 
     Q = [2 + c for c in range(cq)]
     O = [2 + cq + c for c in range(co)]
-    q0, q1 = Q[0], Q[-1]
+    def q(i, rel):
+        step(Q[i], rel)
+
 
     def od(i, rel):
         if i < co:
             step(O[i], rel)
 
     step(0, 0)
-    step(1, 0)
     step_own(0)
     more(acc_k, fk, mate)
+    step(1, 0)
+    step(0, 1)
+    q(0, 0)
+    step(1, 2)
+    step(0, 2)
+    step(0, 3)
+    finish_k()
+    met()
+    spread(0)
+    q(1, 0)
+    q(3, 0)
+    step(1, 3)
+    q(1, 2)
+    step(1, 1)
+    q(1, 1)
+    q(0, 2)
     step_own(1)
     more(acc_v, fv, mate)
-    step(0, 3)
-    step(0, 1)
-    step(0, 2)
-    finish_k()
-    spread(0)
-    step(1, 1)
-    step(1, 2)
-    step(q0, 0)
     step_own(2)
     more(acc_q, fq, mate)
-    step(1, 3)
     finish_v()
     spread(1)
-    collect(0, 2)
-    step(q0, 2)
-    step(q0, 1)
-    step(q1, 0)
-    collect(1, 2)
-    step(q0, 3)
-    step(q1, 2)
+    relay(0, 2)
+    q(3, 1)
+    q(2, 2)
+    q(3, 2)
+    q(0, 1)
+    q(1, 3)
+    od(1, 0)
+    q(2, 0)
+    q(0, 3)
+    od(2, 0)
+    relay(1, 2)
+    od(0, 2)
     finish_q(0)
-    od(0, 0)
-    step(q1, 1)
-    od(1, 0)
-    [collect(0, k) for k in range(1, seqs) if k != 2]
-    [collect(1, k) for k in range(1, seqs) if k != 2]
-    od(2, 0)
-    attend(0, tiles // 4)
-    step(q1, 3)
-    od(3, 0)
-    od(0, 2)
-    attend(tiles // 4, tiles // 2)
-    od(0, 1)
-    od(1, 2)
-    finish_q(1)
-    attend(tiles // 2, tiles * 3 // 4)
+    q(2, 3)
+    q(2, 1)
+    q(3, 3)
+    collect(0)
+    soft(0)
+    od(3, 1)
+    soft(1)
     od(1, 1)
     od(2, 2)
+    finish_q(1)
+    collect(1)
+    blend(0)
+    heads(2)
+    od(0, 0)
+    od(1, 2)
+    od(2, 1)
+    heads(3)
+    od(3, 3)
+    od(3, 0)
+    od(2, 3)
+    od(3, 2)
+    blend(1)
+    od(0, 1)
+    od(0, 3)
     od(1, 3)
-    attend(tiles * 3 // 4, tiles)
-    od(2, 1)
-    od(3, 2)
-    od(2, 3)
     project(d, 0, co)
     step_own(3)
     project(mate, 0, co)
-    od(3, 1)
-    od(3, 3)
-    od(0, 3)
     [project(back(d, j), 0, co) for j in range(1, chips)]
-    for p in O:
-        step_c(p)
+    step_c(3, 0, co)
     for j in range(1, chips):
         project(back(mate, j), 0, co)
     drain()
@@ -381,17 +436,13 @@
     local = tokens.reshape(rows, width)
     chips = n // 2
     kvw, qw = key_weight.shape[1], query_weight.shape[1]
-    cq = 2
+    cq = 4
     co = max(1, min(4, out_weight.shape[1] // LANES))
     pieces = 2 + cq + co
-    Q = range(2, 2 + cq)
-    O = range(2 + cq, pieces)
-    xlist = [(0, 0), (1, 0), (0, 3)] + [(p, r) for p in Q for r in (0, 2)] + [(p, 0) for p in O] + [
-        (p, 3) for p in O[1:]]
-    ylist = [(0, 1), (1, 1), (1, 3)] + [(p, r) for p in Q for r in (1, 3)] + [(p, 1) for p in O]
-    zlist = [(0, 2), (1, 2)] + [(p, 2) for p in O] + [(O[0], 3)]
+    index = {(0, 0): 0, (1, 0): 1, **{(2, c): 2 + c for c in range(cq)}, **{(3, c): 2 + cq + c for c in range(co)}}
+    xlist, ylist, zlist = ([(index[k, c], r) for k, c, r in table if (k, c) in index]
+                           for table in (X_PIECES, Y_PIECES, Z_PIECES))
     route = {**{k: "x" for k in xlist}, **{k: "y" for k in ylist}, **{k: "z" for k in zlist}}
-    zsends = len({p for p, _ in zlist})
     relays = 2 * len([1 for k in range(2, seqs, 2) for o in (1, 2) if k + o < seqs])
     dma = pltpu.SemaphoreType.DMA
     vmem = pl.BlockSpec(memory_space=pltpu.VMEM)
@@ -417,12 +468,13 @@
             pltpu.VMEM((rows, qw), F32),
             pltpu.VMEM((qw // LANES, 2 * rows, LANES), BF),
             pltpu.VMEM((rows, qw), BF),
+            pltpu.VMEM((KV_HEADS // 2, qw // KV_HEADS // HEAD_DIM * rows, seqs * rows), BF),
             dma((7,)), dma((4,)), dma((4,)),
-            dma((chips - 1, pieces)), dma((chips - 1, len(xlist))),
-            dma((chips - 1, pieces)), dma((chips - 1, len(ylist))),
-            dma((chips - 1, zsends)), dma((chips - 1, len(zlist))),
-            dma((chips - 1, pieces)), dma((chips - 1, pieces)),
-            dma((4,)), dma((seqs, 2)), dma((max(1, relays),)),
+            dma((chips - 1, 4)), dma((chips - 1, len(xlist))),
+            dma((chips - 1, 4)), dma((chips - 1, len(ylist))),
+            dma((chips - 1, 4)), dma((chips - 1, len(zlist))),
+            dma((chips - 1, 4)), dma((chips - 1, 5)),
+            dma((4,)), dma((seqs, 2)), dma((max(1, relays),)), pltpu.SemaphoreType.REGULAR((2,)),
         ],
         compiler_params=pltpu.CompilerParams(
             collective_id=0, has_side_effects=True, vmem_limit_bytes=40 * 2 ** 20),

time: 39.8 us -> 36.4 us (0.915)
  Pallas kernels: 38.7 us -> 35.3 us
    pallas_call x1, Pallas kernels: 38.7 us -> 35.3 us  [shards(): pl.pallas_call(functools.partial(kernel, n, groups, seqs, route, xlist, y...]
where the time goes in v2:
time: 36.4 us; the launch traced here: 36.1 us
  Pallas kernels  35.3 us (97%)
  local copies, waits for them, and re-layouts  0.84 us (2%)
    pallas_call x1, Pallas kernels, shards(): pl.pallas_call(functools.partial(kernel, n, groups, seqs, route, xlist, y...  35.3 us
    unnamed x1, local copies, waits for them, and re-layouts  0.84 us

profile of v2, /device:TPU:0, one launch (start us, length us, event | category | flops | bytes accessed | tf_op | source)
XLA Modules:
  0.0 36.1 jit_solution(16614159230962363892)
XLA Ops:
  0.0 35.3 %shard_map.73 = bf16[160,2048]{1,0:T(8,128)(2,1)S(1)} custom-call(bf16[160,2048]{1,0:T(8,128)(2,1)} %bitcast.5, bf16[512,256]{1,0:T(8,128)(2,1)} %wk.1, bf16[512,256]{1,0:T(8,128)(2,1)} %wv.1, bf16[512,1024]{1,0:T(8,128)(2,1)} %wq.1, bf16[1024,512]{1,0:T(8,128)(2,1)} %wo.1, f32[1,64]{1,0:T(1,128)} %bitcast.6, f32[1,64]{1,0:T(1,128)} %bitcast.7), custom_call_target="tpu_custom_call" | custom-call | tf_op jit(solution)/shard_map/pallas_call | solution.py:450
  35.3 0.8 %copy.9 = bf16[1,160,2048]{2,1,0:T(8,128)(2,1)} copy(bf16[1,160,2048]{2,1,0:T(8,128)(2,1)S(1)} %bitcast.4) | data formatting | bytes 1310720

commit v3 on v2

--- a/solution.py
+++ b/solution.py
@@ -39,9 +39,15 @@
 def dot(a, b):
     return jnp.dot(a, b, preferred_element_type=F32)
 
-X_PIECES = ((0, 0, 0), (1, 0, 0), (2, 0, 0), (0, 0, 3), (2, 1, 0), (2, 3, 0), (2, 1, 2), (2, 2, 2), (3, 2, 0), (3, 1, 0), (3, 0, 2), (2, 2, 0), (3, 3, 1), (2, 2, 1), (3, 3, 2), (3, 1, 2), (3, 0, 0), (3, 3, 0), (3, 0, 1))
-Y_PIECES = ((0, 0, 1), (1, 0, 1), (1, 0, 3), (2, 0, 1), (2, 0, 3), (2, 1, 1), (2, 1, 3), (2, 2, 3), (2, 3, 1), (2, 3, 3), (3, 0, 3), (3, 1, 1), (3, 2, 1), (3, 2, 3))
-Z_PIECES = ((0, 0, 2), (1, 0, 2), (2, 0, 2), (2, 3, 2), (3, 1, 3), (3, 2, 2), (3, 3, 3))
+REACH = (2, 3)
+X_PIECES = ((0, 0, 0), (2, 0, 0), (1, 0, 0), (2, 3, 0), (0, 0, 3), (2, 2, 0), (2, 1, 0), (2, 1, 2), (3, 0, 0), (3, 3, 2), (2, 2, 3), (3, 3, 0), (3, 1, 2), (3, 2, 0), (3, 0, 3), (3, 1, 1), (3, 1, 0), (3, 2, 3))
+Y_PIECES = ((0, 0, 1), (1, 0, 1), (1, 0, 3), (2, 0, 1), (2, 0, 3), (2, 1, 1), (2, 1, 3), (2, 2, 1), (2, 3, 1), (2, 3, 3), (3, 0, 1), (3, 1, 3), (3, 2, 1), (3, 3, 1), (3, 3, 3))
+Z_PIECES = ((0, 0, 2), (1, 0, 2), (2, 0, 2), (2, 2, 2), (2, 3, 2), (3, 0, 2), (3, 2, 2))
+
+
+def relays_of(seqs):
+    return [(which, way, k, o) for which in range(2) for way in (1, -1)
+            for k in range(REACH[which], seqs, REACH[which]) for o in range(1, REACH[which] + 1) if k + o < seqs]
 
 
 def kernel(n, groups, seqs, route, xlist, ylist, zlist, cq, co, tok_h, wk, wv, wq, wo, gq_h, gk_h, out,
@@ -79,7 +85,7 @@
 
     e = lax.rem(s, 2)
     colors = (2 * g + e, 2 * other(g) + e, 2 * g + other(e), 2 * other(g) + other(e))
-    offsets = (2, -2, 1, -1)
+    offsets = tuple(way * o for o in range(max(REACH), 0, -1) for way in (1, -1))
 
     barrier = pltpu.get_barrier_semaphore()
     for j in range(1, chips):
@@ -126,10 +132,19 @@
         copy.wait()
     pl.semaphore_wait(barrier, count)
 
-    for i, o in enumerate((1, -1)):
-        def vouch(i=i, o=o):
-            pl.semaphore_signal(ready.at[i], inc=1, device_id={"sp": near(s + o)}, device_id_type=MESH)
-        pl.when(inside(s + o) & inside(s - o))(vouch)
+    def vouch(level):
+        for i, o in enumerate((1, -1)):
+            def tell(i=i, o=o):
+                pl.semaphore_signal(ready.at[level - 1, i], inc=1, device_id={"sp": near(s + o)}, device_id_type=MESH)
+            pl.when(inside(s + o) & inside(s - level * o))(tell)
+
+    def heard(level):
+        for i, o in enumerate((1, -1)):
+            def wait(i=i):
+                pl.semaphore_wait(ready.at[level - 1, i], 1)
+            pl.when(inside(s - o) & inside(s - (level + 1) * o))(wait)
+
+    vouch(1)
 
     def x_send(index):
         p, rel = xlist[index]
@@ -185,56 +200,67 @@
                 here = full[kind].at[d]
                 remote(here, here, cs.at[j - 1, kind], cr.at[j - 1, 0], {"dp": mate}).wait_send()
         for i, o in enumerate(offsets):
-            here = kv.at[s]
+            uses = [which for which in range(2) if abs(o) <= REACH[which]]
+            here = kv.at[s] if len(uses) == 2 else slot(s, uses[0])
             pl.when(inside(s + o))(remote(here, here, hs.at[i], hr.at[0, 0], {"dp": mate}).wait_send)
-        for i, (way, k, o) in enumerate(relays):
-            here = kv.at[near(s - way * k)]
+        for i, (which, way, k, o) in enumerate(relays):
+            here = slot(near(s - way * k), which)
             pl.when(inside(s - way * k) & inside(s + way * o))(
                 remote(here, here, fs.at[i], hr.at[0, 0], {"dp": mate}).wait_send)
 
-    relays = [(way, k, o) for way in (1, -1) for k in range(2, seqs, 2) for o in (1, 2) if k + o < seqs]
+    relays = relays_of(seqs)
     half = kv.shape[2] // 2
 
     def slot(i, which):
         return kv.at[i, :, pl.ds(which * half, half)]
 
-    def met():
-        for i, o in enumerate((1, -1)):
-            def heard(i=i):
-                pl.semaphore_wait(ready.at[i], 1)
-            pl.when(inside(s - o) & inside(s - 2 * o))(heard)
+    known = []
+
+    def meet(level):
+        while len(known) < level:
+            heard(len(known) + 1)
+            if len(known) + 2 < max(REACH):
+                vouch(len(known) + 2)
+            known.append(level)
 
     def spread(which):
+        meet(REACH[which] - 1)
+        here = slot(s, which)
         for i, o in enumerate(offsets):
-            here = slot(s, which)
-            pl.when(inside(s + o))(
-                remote(here, here, hs.at[i], hr.at[s, which], {"sp": near(s + o)}).start)
-
-    def onward(way, k):
-        return functools.reduce(lambda a, b: a | b, [inside(s + way * o) for w, kk, o in relays if (w, kk) == (way, k)])
+            if abs(o) <= REACH[which]:
+                pl.when(inside(s + o))(
+                    remote(here, here, hs.at[i], hr.at[s, which], {"sp": near(s + o)}).start)
+
+    def onward(which, way, k):
+        return functools.reduce(lambda a, b: a | b, [
+            inside(s + way * o) for i, w, kk, o in relays if (i, w, kk) == (which, way, k)])
 
     def take(which, way, k):
         source = near(s - way * k)
         arrive(slot(source, which), hs.at[0], hr.at[source, which])
 
-    def relay(which, k):
-        for way in (1, -1):
-            if not [1 for w, kk, o in relays if (w, kk) == (way, k)]:
-                continue
-            source = near(s - way * k)
-            here = slot(source, which)
-            pl.when(inside(s - way * k) & onward(way, k))(functools.partial(take, which, way, k))
-            for i, (w, kk, o) in enumerate(relays):
-                if (w, kk) == (way, k):
-                    pl.when(inside(s - way * k) & inside(s + way * o))(
-                        remote(here, here, fs.at[i], hr.at[source, which], {"sp": near(s + way * o)}).start)
+    def relayed(which, way, k):
+        return bool([1 for i, w, kk, o in relays if (i, w, kk) == (which, way, k)])
+
+    def relay(which):
+        for k in range(REACH[which], seqs, REACH[which]):
+            for way in (1, -1):
+                if not relayed(which, way, k):
+                    continue
+                source = near(s - way * k)
+                here = slot(source, which)
+                pl.when(inside(s - way * k) & onward(which, way, k))(functools.partial(take, which, way, k))
+                for i, (kind, w, kk, o) in enumerate(relays):
+                    if (kind, w, kk) == (which, way, k):
+                        pl.when(inside(s - way * k) & inside(s + way * o))(
+                            remote(here, here, fs.at[i], hr.at[source, which], {"sp": near(s + way * o)}).start)
 
     def collect(which):
         for k in range(1, seqs):
             for way in (1, -1):
                 need = inside(s - way * k)
-                if [1 for w, kk, o in relays if (w, kk) == (way, k)]:
-                    need = need & jnp.logical_not(onward(way, k))
+                if relayed(which, way, k):
+                    need = need & jnp.logical_not(onward(which, way, k))
                 pl.when(need)(functools.partial(take, which, way, k))
 
     depth = fq.shape[1]
@@ -253,77 +279,101 @@
     first(acc_q, fq)
 
     lane = lax.broadcasted_iota(jnp.int32, (rows, LANES), 1)
-    low_half = lax.rem(lane, HEAD_DIM) < HEAD_DIM // 2
     low_head = lane < HEAD_DIM
     square_r = lax.broadcasted_iota(jnp.int32, (LANES, LANES), 0)
     square_c = lax.broadcasted_iota(jnp.int32, (LANES, LANES), 1)
     same_head = jnp.where(square_r // HEAD_DIM == square_c // HEAD_DIM, 1.0, 0.0).astype(BF)
 
+    twice_head = jnp.concatenate([same_head] * 2, axis=0)
+
+    def halves(a, b):
+        middle = a.shape[0] // 32 * 16
+        return jnp.concatenate([dot(a[:middle], b), dot(a[middle:], b)], axis=0)
+
     gain_k = jnp.concatenate([gk[...]] * 2, axis=1)
-    gain_q = jnp.concatenate([gq[...]] * 2, axis=1)
-
-    def norm_rotate(raw, gain):
+    gain_q = jnp.concatenate([gq[...]] * 2, axis=1) * HEAD_DIM ** (-0.5)
+
+    def norm_rotate(acc, tiles_, gain):
+        raw = jnp.concatenate([acc[:, pl.ds(t * LANES, LANES)] for t in tiles_], axis=0)
+        many = raw.shape[0]
         sq = raw * raw
         high = sq.astype(BF)
         low = (sq - high.astype(F32)).astype(BF)
-        total = dot(high, same_head) + dot(low, same_head)
+        total = halves(jnp.concatenate([high, low], axis=1), twice_head)
         scaled = raw * lax.rsqrt(total * (1.0 / HEAD_DIM) + norm_eps) * gain
-        other = jnp.where(low_half, pltpu.roll(scaled, LANES - HEAD_DIM // 2, 1),
-                          pltpu.roll(scaled, HEAD_DIM // 2, 1))
-        return scaled * cos[...] + other * sin[...]
+        lanes = lax.broadcasted_iota(jnp.int32, (many, LANES), 1)
+        other = jnp.where(lax.rem(lanes, HEAD_DIM) < HEAD_DIM // 2,
+                          pltpu.roll(scaled, LANES - HEAD_DIM // 2, 1), pltpu.roll(scaled, HEAD_DIM // 2, 1))
+        again = len(tiles_)
+        return scaled * jnp.concatenate([cos[...]] * again, axis=0) + other * jnp.concatenate([sin[...]] * again, axis=0)
 
     others = [(d, j) for j in range(1, chips)] + [(mate, j) for j in range(1, chips)]
 
     def finish_k():
+        for j in range(1, chips):
+            more(acc_k, fk, back(d, j))
         step_c(0, 0, 1)
-        for dev, j in others:
-            more(acc_k, fk, back(dev, j))
+        for j in range(1, chips):
+            more(acc_k, fk, back(mate, j))
+        turned = norm_rotate(acc_k, range(half // LANES), gain_k).astype(BF)
         for t in range(half // LANES):
-            cols = pl.ds(t * LANES, LANES)
-            kv[s, :, cols] = norm_rotate(acc_k[:, cols], gain_k).astype(BF)
+            kv[s, :, pl.ds(t * LANES, LANES)] = turned[t * rows:(t + 1) * rows]
 
     def finish_v():
+        for j in range(1, chips):
+            more(acc_v, fv, back(d, j))
         step_c(1, 0, 1)
-        for dev, j in others:
-            more(acc_v, fv, back(dev, j))
+        for j in range(1, chips):
+            more(acc_v, fv, back(mate, j))
         kv[s, :, pl.ds(half, half)] = acc_v[...].astype(BF)
 
     tiles = fq.shape[2] // LANES
     group = HEADS // KV_HEADS
 
     def finish_q(part_):
-        step_c(2, part_ * cq // 2, (part_ + 1) * cq // 2)
         width = fq.shape[2] // 2
         cols = pl.ds(part_ * width, width)
+        step_c(2, part_ * cq // 2, (part_ + 1) * cq // 2)
         for dev, j in others:
-            owner = back(dev, j)
-            acc_q[:, cols] += dot(tok[:, columns(owner)], fq[owner, :, cols])
-        for t in range(part_ * tiles // 2, (part_ + 1) * tiles // 2):
-            turned = norm_rotate(acc_q[:, pl.ds(t * LANES, LANES)], gain_q * HEAD_DIM ** (-0.5))
-            swapped = pltpu.roll(turned, HEAD_DIM, 1)
+            acc_q[:, cols] += dot(tok[:, columns(back(dev, j))], fq[back(dev, j), :, cols])
+        mine = range(part_ * tiles // 2, (part_ + 1) * tiles // 2)
+        turned = norm_rotate(acc_q, mine, gain_q)
+        swapped = pltpu.roll(turned, HEAD_DIM, 1)
+        for i, t in enumerate(mine):
+            here, there = turned[i * rows:(i + 1) * rows], swapped[i * rows:(i + 1) * rows]
             if (2 * t // group) % 2 == 0:
-                one, two = jnp.where(low_head, turned, 0.0), jnp.where(low_head, swapped, 0.0)
+                one, two = jnp.where(low_head, here, 0.0), jnp.where(low_head, there, 0.0)
             else:
-                one, two = jnp.where(low_head, 0.0, swapped), jnp.where(low_head, 0.0, turned)
+                one, two = jnp.where(low_head, 0.0, there), jnp.where(low_head, 0.0, here)
             qs[t, pl.ds(0, rows), :] = one.astype(BF)
             qs[t, pl.ds(rows, rows), :] = two.astype(BF)
 
-    def softmax(h):
+    def soft(h):
         base = (h // 2) * LANES
         keys = kv[:, :, pl.ds(base, LANES)].reshape(seqs * rows, LANES)
         lo, count = h * tiles // KV_HEADS, tiles // KV_HEADS
         asked = qs[lo:lo + count].reshape(count * 2 * rows, LANES)
-        scores = lax.dot_general(asked, keys, (((1,), (1,)), ((), ())), preferred_element_type=F32)
-        top = jnp.max(scores, axis=-1, keepdims=True)
-        weights = jnp.exp(scores - top)
-        inverse = 1.0 / jnp.sum(weights, axis=-1, keepdims=True)
-        return (weights * inverse).astype(BF)
+        blocks = 4
+        size = count * 2 * rows // blocks
+        def score(i):
+            return lax.dot_general(asked[i * size:(i + 1) * size], keys, (((1,), (1,)), ((), ())),
+                                   preferred_element_type=F32)
+
+        following = score(0)
+        for i in range(blocks):
+            scores = following
+            if i + 1 < blocks:
+                following = score(i + 1)
+            top = jnp.max(scores, axis=-1, keepdims=True)
+            weights = jnp.exp(scores - top)
+            inverse = 1.0 / jnp.sum(weights, axis=-1, keepdims=True)
+            probs[h, i * size:(i + 1) * size, :] = (weights * inverse).astype(BF)
 
     def mix(h, weights):
         base = (h // 2) * LANES
         lo, count = h * tiles // KV_HEADS, tiles // KV_HEADS
         values = kv[:, :, pl.ds(half + base, LANES)].reshape(seqs * rows, LANES)
-        mixed = dot(weights, values)
+        mixed = halves(weights, values)
         for i in range(count):
             one, two = mixed[2 * i * rows:(2 * i + 1) * rows], mixed[(2 * i + 1) * rows:(2 * i + 2) * rows]
             if h % 2 == 0:
@@ -332,14 +382,8 @@
                 one = pltpu.roll(one, HEAD_DIM, 1)
             att[:, pl.ds((lo + i) * LANES, LANES)] = jnp.where(low_head, one, two).astype(BF)
 
-    def soft(h):
-        probs[h] = softmax(h)
-
     def blend(h):
         mix(h, probs[h])
-
-    def heads(h):
-        mix(h, softmax(h))
 
     def project(owner, lo, hi):
         width = fo.shape[2]
@@ -359,68 +403,70 @@
             step(O[i], rel)
 
     step(0, 0)
+    meet(1)
+    q(0, 0)
+    step_own(2)
+    more(acc_q, fq, mate)
+    step(1, 0)
+    q(3, 0)
+    step(0, 1)
+    q(0, 2)
     step_own(0)
     more(acc_k, fk, mate)
-    step(1, 0)
-    step(0, 1)
-    q(0, 0)
+    step_own(1)
+    more(acc_v, fv, mate)
+    step(0, 3)
     step(1, 2)
     step(0, 2)
-    step(0, 3)
     finish_k()
-    met()
     spread(0)
-    q(1, 0)
-    q(3, 0)
-    step(1, 3)
+    q(2, 0)
+    q(3, 2)
     q(1, 2)
     step(1, 1)
-    q(1, 1)
-    q(0, 2)
-    step_own(1)
-    more(acc_v, fv, mate)
-    step_own(2)
-    more(acc_q, fq, mate)
+    q(0, 3)
+    relay(0)
+    q(1, 0)
+    step(1, 3)
     finish_v()
     spread(1)
-    relay(0, 2)
-    q(3, 1)
-    q(2, 2)
-    q(3, 2)
+    q(2, 3)
+    od(0, 0)
+    od(3, 0)
     q(0, 1)
     q(1, 3)
-    od(1, 0)
-    q(2, 0)
-    q(0, 3)
+    q(2, 2)
+    q(3, 1)
+    q(1, 1)
+    q(3, 3)
+    od(3, 2)
+    q(2, 1)
+    finish_q(0)
+    finish_q(1)
+    od(1, 2)
     od(2, 0)
-    relay(1, 2)
-    od(0, 2)
-    finish_q(0)
-    q(2, 3)
-    q(2, 1)
-    q(3, 3)
+    relay(1)
     collect(0)
     soft(0)
+    soft(2)
+    soft(1)
     od(3, 1)
-    soft(1)
+    soft(3)
+    collect(1)
+    blend(2)
+    blend(0)
+    od(0, 3)
+    od(0, 1)
+    od(3, 3)
+    od(0, 2)
     od(1, 1)
+    blend(1)
+    od(2, 3)
+    od(2, 1)
+    od(1, 3)
+    od(1, 0)
+    blend(3)
     od(2, 2)
-    finish_q(1)
-    collect(1)
-    blend(0)
-    heads(2)
-    od(0, 0)
-    od(1, 2)
-    od(2, 1)
-    heads(3)
-    od(3, 3)
-    od(3, 0)
-    od(2, 3)
-    od(3, 2)
-    blend(1)
-    od(0, 1)
-    od(0, 3)
-    od(1, 3)
     project(d, 0, co)
     step_own(3)
     project(mate, 0, co)
@@ -443,7 +489,6 @@
     xlist, ylist, zlist = ([(index[k, c], r) for k, c, r in table if (k, c) in index]
                            for table in (X_PIECES, Y_PIECES, Z_PIECES))
     route = {**{k: "x" for k in xlist}, **{k: "y" for k in ylist}, **{k: "z" for k in zlist}}
-    relays = 2 * len([1 for k in range(2, seqs, 2) for o in (1, 2) if k + o < seqs])
     dma = pltpu.SemaphoreType.DMA
     vmem = pl.BlockSpec(memory_space=pltpu.VMEM)
     hbm = pl.BlockSpec(memory_space=pltpu.HBM)
@@ -468,13 +513,14 @@
             pltpu.VMEM((rows, qw), F32),
             pltpu.VMEM((qw // LANES, 2 * rows, LANES), BF),
             pltpu.VMEM((rows, qw), BF),
-            pltpu.VMEM((KV_HEADS // 2, qw // KV_HEADS // HEAD_DIM * rows, seqs * rows), BF),
+            pltpu.VMEM((KV_HEADS, qw // KV_HEADS // HEAD_DIM * rows, seqs * rows), BF),
             dma((7,)), dma((4,)), dma((4,)),
             dma((chips - 1, 4)), dma((chips - 1, len(xlist))),
             dma((chips - 1, 4)), dma((chips - 1, len(ylist))),
             dma((chips - 1, 4)), dma((chips - 1, len(zlist))),
             dma((chips - 1, 4)), dma((chips - 1, 5)),
-            dma((4,)), dma((seqs, 2)), dma((max(1, relays),)), pltpu.SemaphoreType.REGULAR((2,)),
+            dma((2 * max(REACH),)), dma((seqs, 2)), dma((max(1, len(relays_of(seqs))),)),
+            pltpu.SemaphoreType.REGULAR((max(REACH) - 1, 2)),
         ],
         compiler_params=pltpu.CompilerParams(
             collective_id=0, has_side_effects=True, vmem_limit_bytes=40 * 2 ** 20),

time: 36.4 us -> 35.5 us (0.975)
  Pallas kernels: 35.3 us -> 34.5 us
    pallas_call x1, Pallas kernels: 35.3 us -> 34.5 us  [shards(): pl.pallas_call(functools.partial(kernel, n, groups, seqs, route, xlist, y...]
where the time goes in v3:
time: 35.5 us; the launch traced here: 35.3 us
  Pallas kernels  34.5 us (97%)
  local copies, waits for them, and re-layouts  0.84 us (2%)
    pallas_call x1, Pallas kernels, shards(): pl.pallas_call(functools.partial(kernel, n, groups, seqs, route, xlist, y...  34.5 us
    unnamed x1, local copies, waits for them, and re-layouts  0.84 us

profile of v3, /device:TPU:0, one launch (start us, length us, event | category | flops | bytes accessed | tf_op | source)
XLA Modules:
  0.0 35.3 jit_solution(16503571905220711380)
XLA Ops:
  0.0 34.5 %shard_map.73 = bf16[160,2048]{1,0:T(8,128)(2,1)S(1)} custom-call(bf16[160,2048]{1,0:T(8,128)(2,1)} %bitcast.5, bf16[512,256]{1,0:T(8,128)(2,1)} %wk.1, bf16[512,256]{1,0:T(8,128)(2,1)} %wv.1, bf16[512,1024]{1,0:T(8,128)(2,1)} %wq.1, bf16[1024,512]{1,0:T(8,128)(2,1)} %wo.1, f32[1,64]{1,0:T(1,128)} %bitcast.6, f32[1,64]{1,0:T(1,128)} %bitcast.7), custom_call_target="tpu_custom_call" | custom-call | tf_op jit(solution)/shard_map/pallas_call | solution.py:495
  34.5 0.8 %copy.9 = bf16[1,160,2048]{2,1,0:T(8,128)(2,1)} copy(bf16[1,160,2048]{2,1,0:T(8,128)(2,1)S(1)} %bitcast.4) | data formatting | bytes 1310720

commit v4 on v3

--- a/solution.py
+++ b/solution.py
@@ -52,7 +52,7 @@
 
 def kernel(n, groups, seqs, route, xlist, ylist, zlist, cq, co, tok_h, wk, wv, wq, wo, gq_h, gk_h, out,
            fk, fv, fq, fo, tok, gq, gk, cos, sin, kv, acc_k, acc_v, acc_q, qs, att, probs,
-           ls, os_, or_, xs, xr, ys, yr, zs, zr, cs, cr, hs, hr, fs, ready):
+           ls, os_, or_, ws, xr, yr, zr, cs, cr, hr, fs, ready):
     d = lax.axis_index("dp")
     g = lax.axis_index("grp")
     s = lax.axis_index("sp")
@@ -62,11 +62,17 @@
     rows = tok.shape[0]
 
     loads = []
-    for i, (src, dst) in enumerate(((wk, fk.at[d]), (wv, fv.at[d]), (tok_h, tok), (wq, fq.at[d]), (wo, fo.at[d]),
+    for i, (src, dst) in enumerate(((wk, fk.at[d]), (wv, fv.at[d]), (wq, fq.at[d]), (wo, fo.at[d]), (tok_h, tok),
                                     (gq_h, gq), (gk_h, gk))):
-        copy = pltpu.make_async_copy(src, dst, ls.at[i])
-        copy.start()
-        loads.append(copy)
+        loads.append(pltpu.make_async_copy(src, dst, ls.at[i]))
+    for i in (0, 2, 1, 3, 4, 5, 6):
+        loads[i].start()
+    there = []
+
+    def need(i):
+        if i not in there:
+            there.append(i)
+            loads[i].wait()
 
     def hop(j):
         return lax.rem(d + 2 * j, n)
@@ -128,8 +134,7 @@
     def held(owner, p, rel):
         return part(owner, p, colors[rel], 1)
 
-    for copy in loads:
-        copy.wait()
+    need(0)
     pl.semaphore_wait(barrier, count)
 
     def vouch(level):
@@ -148,13 +153,15 @@
 
     def x_send(index):
         p, rel = xlist[index]
+        need(pieces[p][0])
         for j in range(1, chips):
             here = held(d, p, rel)
-            remote(here, here, xs.at[j - 1, pieces[p][0]], xr.at[j - 1, index], {"dp": hop(j)}).start()
+            remote(here, here, ws.at[j - 1], xr.at[j - 1, index], {"dp": hop(j)}).start()
 
     def own_send(kind):
+        need(kind)
         here = full[kind].at[d]
-        remote(here, here, os_.at[kind], or_.at[kind], {"dp": mate}).start()
+        remote(here, here, os_.at[0], or_.at[kind], {"dp": mate}).start()
 
     for index in range(4):
         x_send(index)
@@ -165,44 +172,39 @@
 
     def step(p, rel):
         way = route[p, rel]
-        table, ssem, rsem = {"x": (xlist, xs, xr), "y": (ylist, ys, yr), "z": (zlist, zs, zr)}[way]
+        table, rsem = {"x": (xlist, xr), "y": (ylist, yr), "z": (zlist, zr)}[way]
         for j in range(1, chips):
             here = held(back(d, j), p, rel)
-            arrive(here, ssem.at[j - 1, 0], rsem.at[j - 1, table.index((p, rel))])
+            arrive(here, ws.at[j - 1], rsem.at[j - 1, table.index((p, rel))])
             if rel in (0, 1) and route[p, rel + 2] == "z":
                 i = zlist.index((p, rel + 2))
-                remote(here, here, zs.at[j - 1, pieces[p][0]], zr.at[j - 1, i], {"sp": other(s)}).start()
+                remote(here, here, ws.at[j - 1], zr.at[j - 1, i], {"sp": other(s)}).start()
             if rel in (0, 2) and route[p, rel + 1] == "y":
                 i = ylist.index((p, rel + 1))
-                remote(here, here, ys.at[j - 1, pieces[p][0]], yr.at[j - 1, i], {"grp": other(g)}).start()
-            remote(here, here, cs.at[j - 1, pieces[p][0]], cr.at[j - 1, shelf[p]], {"dp": mate}).start()
+                remote(here, here, ws.at[j - 1], yr.at[j - 1, i], {"grp": other(g)}).start()
+            remote(here, here, cs.at[j - 1], cr.at[j - 1, shelf[p]], {"dp": mate}).start()
 
     def step_c(kind, lo, hi):
         width = full[kind].shape[2] // cuts[kind]
         for j in range(1, chips):
             arrive(full[kind].at[back(mate, j), :, pl.ds(lo * width, (hi - lo) * width)],
-                   cs.at[j - 1, kind], cr.at[j - 1, shelf[pieces.index((kind, lo))]])
+                   cs.at[j - 1], cr.at[j - 1, shelf[pieces.index((kind, lo))]])
 
     def step_own(kind):
-        arrive(full[kind].at[mate], os_.at[kind], or_.at[kind])
+        arrive(full[kind].at[mate], os_.at[0], or_.at[kind])
 
     def drain():
-        for kind in range(4):
-            here = full[kind].at[d]
-            remote(here, here, os_.at[kind], or_.at[kind], {"dp": mate}).wait_send()
-        for j in range(1, chips):
-            for kind in range(4):
-                for table, sem in ((xlist, xs), (ylist, ys), (zlist, zs)):
-                    blocks = len([1 for q, _ in table if pieces[q][0] == kind])
-                    if blocks:
-                        here = full[kind].at[d, pl.ds(0, blocks * (full[kind].shape[1] // 4) // cuts[kind])]
-                        remote(here, here, sem.at[j - 1, kind], xr.at[0, 0], {"dp": mate}).wait_send()
-                here = full[kind].at[d]
-                remote(here, here, cs.at[j - 1, kind], cr.at[j - 1, 0], {"dp": mate}).wait_send()
+        total = sum(ref.shape[1] * ref.shape[2] for ref in full) // fq.shape[2]
+        parts = [a for a in range(1, n + 1) if total % (16 * a) == 0 and total // a <= fq.shape[1]][0]
+        here = fq.at[pl.ds(0, parts), pl.ds(0, total // parts)]
+        remote(here, here, os_.at[0], or_.at[0], {"dp": mate}).wait_send()
+        for j in range(1, chips):
+            for sem in (ws, cs):
+                remote(here, here, sem.at[j - 1], or_.at[0], {"dp": mate}).wait_send()
         for i, o in enumerate(offsets):
             uses = [which for which in range(2) if abs(o) <= REACH[which]]
             here = kv.at[s] if len(uses) == 2 else slot(s, uses[0])
-            pl.when(inside(s + o))(remote(here, here, hs.at[i], hr.at[0, 0], {"dp": mate}).wait_send)
+            pl.when(inside(s + o))(remote(here, here, ls.at[i], hr.at[0, 0], {"dp": mate}).wait_send)
         for i, (which, way, k, o) in enumerate(relays):
             here = slot(near(s - way * k), which)
             pl.when(inside(s - way * k) & inside(s + way * o))(
@@ -229,7 +231,7 @@
         for i, o in enumerate(offsets):
             if abs(o) <= REACH[which]:
                 pl.when(inside(s + o))(
-                    remote(here, here, hs.at[i], hr.at[s, which], {"sp": near(s + o)}).start)
+                    remote(here, here, ls.at[i], hr.at[s, which], {"sp": near(s + o)}).start)
 
     def onward(which, way, k):
         return functools.reduce(lambda a, b: a | b, [
@@ -237,7 +239,7 @@
 
     def take(which, way, k):
         source = near(s - way * k)
-        arrive(slot(source, which), hs.at[0], hr.at[source, which])
+        arrive(slot(source, which), ls.at[0], hr.at[source, which])
 
     def relayed(which, way, k):
         return bool([1 for i, w, kk, o in relays if (i, w, kk) == (which, way, k)])
@@ -274,6 +276,8 @@
     def more(acc, ref, owner):
         acc[...] += dot(tok[:, columns(owner)], ref[owner])
 
+    for i in range(len(loads)):
+        need(i)
     first(acc_k, fk)
     first(acc_v, fv)
     first(acc_q, fq)
@@ -514,12 +518,9 @@
             pltpu.VMEM((qw // LANES, 2 * rows, LANES), BF),
             pltpu.VMEM((rows, qw), BF),
             pltpu.VMEM((KV_HEADS, qw // KV_HEADS // HEAD_DIM * rows, seqs * rows), BF),
-            dma((7,)), dma((4,)), dma((4,)),
-            dma((chips - 1, 4)), dma((chips - 1, len(xlist))),
-            dma((chips - 1, 4)), dma((chips - 1, len(ylist))),
-            dma((chips - 1, 4)), dma((chips - 1, len(zlist))),
-            dma((chips - 1, 4)), dma((chips - 1, 5)),
-            dma((2 * max(REACH),)), dma((seqs, 2)), dma((max(1, len(relays_of(seqs))),)),
+            dma((7,)), dma((1,)), dma((4,)), dma((chips - 1,)), dma((chips - 1, len(xlist))),
+            dma((chips - 1, len(ylist))), dma((chips - 1, len(zlist))), dma((chips - 1,)), dma((chips - 1, 5)),
+            dma((seqs, 2)), dma((max(1, len(relays_of(seqs))),)),
             pltpu.SemaphoreType.REGULAR((max(REACH) - 1, 2)),
         ],
         compiler_params=pltpu.CompilerParams(

time: 35.5 us -> 34.9 us (0.983)
  Pallas kernels: 34.5 us -> 33.9 us
    pallas_call x1, Pallas kernels: 34.5 us -> 33.9 us  [shards(): pl.pallas_call(functools.partial(kernel, n, groups, seqs, route, xlist, y...]
where the time goes in v4:
time: 34.9 us; the launch traced here: 34.7 us
  Pallas kernels  33.9 us (97%)
  local copies, waits for them, and re-layouts  0.84 us (2%)
    pallas_call x1, Pallas kernels, shards(): pl.pallas_call(functools.partial(kernel, n, groups, seqs, route, xlist, y...  33.9 us
    unnamed x1, local copies, waits for them, and re-layouts  0.84 us

profile of v4, /device:TPU:0, one launch (start us, length us, event | category | flops | bytes accessed | tf_op | source)
XLA Modules:
  0.0 34.7 jit_solution(16901504280332834833)
XLA Ops:
  0.0 33.9 %shard_map.73 = bf16[160,2048]{1,0:T(8,128)(2,1)S(1)} custom-call(bf16[160,2048]{1,0:T(8,128)(2,1)} %bitcast.5, bf16[512,256]{1,0:T(8,128)(2,1)} %wk.1, bf16[512,256]{1,0:T(8,128)(2,1)} %wv.1, bf16[512,1024]{1,0:T(8,128)(2,1)} %wq.1, bf16[1024,512]{1,0:T(8,128)(2,1)} %wo.1, f32[1,64]{1,0:T(1,128)} %bitcast.6, f32[1,64]{1,0:T(1,128)} %bitcast.7), custom_call_target="tpu_custom_call" | custom-call | tf_op jit(solution)/shard_map/pallas_call | solution.py:499
  33.9 0.8 %copy.9 = bf16[1,160,2048]{2,1,0:T(8,128)(2,1)} copy(bf16[1,160,2048]{2,1,0:T(8,128)(2,1)S(1)} %bitcast.4) | data formatting | bytes 1310720
